TPU v7x, 128 devices: a whole 4x4x4 slice. The times are simulated.
128 devices in a mesh: sp: 16 (over z, y), tp: 8 (over x, core).
Axes of the slice: x: 4, y: 4, z: 4, core: 2. Of those that a mesh axis runs over, the one named last changes fastest.
Arguments:
- tokens: bfloat16 [12288, 2048], P('sp'), may hold values from -6 to 6
- norm_gain: float32 [2048], replicated, may hold values from 0.5 to 80
- grid_query_weight: bfloat16 [2048, 2048], P(None, 'tp'), may hold values from -0.5 to 0.5
- grid_key_weight: bfloat16 [2048, 1024], P(None, 'tp'), may hold values from -0.5 to 0.5
- grid_value_weight: bfloat16 [2048, 1024], P(None, 'tp'), may hold values from -0.5 to 0.5
- grid_query_gain: float32 [128], replicated, may hold values from 1.6 to 6
- grid_key_gain: float32 [128], replicated, may hold values from 1.6 to 6
- local_query_weight: bfloat16 [2048, 2048], P(None, 'tp'), may hold values from -0.5 to 0.5
- local_key_weight: bfloat16 [2048, 1024], P(None, 'tp'), may hold values from -0.5 to 0.5
- local_value_weight: bfloat16 [2048, 1024], P(None, 'tp'), may hold values from -0.5 to 0.5
- sink_logit: float32 [16], P('tp'), may hold values from 1 to 6
- grid_out_weight: bfloat16 [2048, 2048], P('tp'), may hold values from -0.09375 to 0.09375
- local_out_weight: bfloat16 [2048, 2048], P('tp'), may hold values from -0.09375 to 0.09375
Outputs:
- mixed: bfloat16 [12288, 2048], P(('sp', 'tp'))
All inputs are finite; a program needn't handle non-finite values.
Results may differ from a plain program's by a relative error of at most 0.03.
Values may be sent and summed in bfloat16 or wider, within the bound.
A program may use at most 192 MiB of HBM per device.

v0:
```python
import jax
import jax.numpy as jnp
from jax import lax
from jax.sharding import PartitionSpec as P

HEAD = 128
WINDOW = 128
GRID_W = 64


EPSILON = 1e-06
ROPE_BASE = 10000.0


def padded(block, sides, width):
    for axis, dim in sides:
        count = lax.axis_size(axis)
        forward = [(i, i + 1) for i in range(count - 1)]
        backward = [(target, source) for source, target in forward]
        low = lax.ppermute(
            lax.slice_in_dim(block, block.shape[dim] - width, None, axis=dim), axis, forward
        )
        high = lax.ppermute(lax.slice_in_dim(block, 0, width, axis=dim), axis, backward)
        block = jnp.concatenate([low, block, high], axis=dim)
    return block


def rms_rows(values, gain):
    widened = values.astype(jnp.float32)
    return widened * lax.rsqrt(jnp.mean(widened * widened, axis=-1, keepdims=True) + EPSILON) * gain


def half_turn(part, angles):
    cosine = jnp.cos(angles)
    sine = jnp.sin(angles)
    cosine = jnp.concatenate([cosine, cosine], axis=-1)
    sine = jnp.concatenate([sine, sine], axis=-1)
    first, second = jnp.split(part, 2, axis=-1)
    turned = jnp.concatenate([-second, first], axis=-1)
    return part * cosine + turned * sine


def axial_turn(heads, positions):
    half_dim = heads.shape[-1] // 2
    inverse = ROPE_BASE ** (-jnp.arange(0, half_dim, 2, dtype=jnp.float32) / half_dim)
    row_angle = (positions // GRID_W).astype(jnp.float32)[:, None, None] * inverse
    col_angle = (positions % GRID_W).astype(jnp.float32)[:, None, None] * inverse
    return jnp.concatenate(
        [half_turn(heads[..., :half_dim], row_angle), half_turn(heads[..., half_dim:], col_angle)],
        axis=-1,
    )


def shards(
    tokens,
    norm_gain,
    grid_query_weight,
    grid_key_weight,
    grid_value_weight,
    grid_query_gain,
    grid_key_gain,
    local_query_weight,
    local_key_weight,
    local_value_weight,
    sink_logit,
    grid_out_weight,
    local_out_weight,
):
    row_count = tokens.shape[0]
    seq_devices = lax.axis_size("sp")
    total_rows = row_count * seq_devices
    offset = lax.axis_index("sp") * row_count
    positions = offset + jnp.arange(row_count, dtype=jnp.int32)
    normed = rms_rows(tokens, norm_gain).astype(jnp.bfloat16)
    score_scale = HEAD ** (-0.5)
    width = grid_out_weight.shape[1]

    def project(weight):
        return jnp.dot(normed, weight, preferred_element_type=jnp.float32).astype(jnp.bfloat16)

    grid_heads = grid_query_weight.shape[1] // HEAD
    grid_groups = grid_key_weight.shape[1] // HEAD
    group_size = grid_heads // grid_groups
    queries = (
        axial_turn(
            rms_rows(
                project(grid_query_weight).reshape(row_count, grid_heads, HEAD), grid_query_gain
            ),
            positions,
        )
        .astype(jnp.bfloat16)
        .reshape(row_count, grid_groups, group_size, HEAD)
    )
    keys = axial_turn(
        rms_rows(project(grid_key_weight).reshape(row_count, grid_groups, HEAD), grid_key_gain),
        positions,
    ).astype(jnp.bfloat16)
    values = project(grid_value_weight).reshape(row_count, grid_groups, HEAD)
    running = jnp.full((grid_groups, group_size, row_count), -jnp.inf, jnp.float32)
    totals = jnp.zeros((grid_groups, group_size, row_count), jnp.float32)
    summed = jnp.zeros((grid_groups, group_size, row_count, HEAD), jnp.float32)
    scores = (
        jnp.einsum(
            "qhgd,shd->hgqs",
            queries,
            lax.all_gather(keys, "sp", axis=0, tiled=True),
            preferred_element_type=jnp.float32,
        )
        * score_scale
    )
    highest = jnp.max(scores, axis=-1)
    factor = jnp.exp(running - highest)
    weights = jnp.exp(scores - highest[..., None])
    totals = totals * factor + jnp.sum(weights, axis=-1)
    summed = summed * factor[..., None] + jnp.einsum(
        "hgqs,shd->hgqd",
        weights.astype(jnp.bfloat16),
        lax.all_gather(values, "sp", axis=0, tiled=True),
        preferred_element_type=jnp.float32,
    )
    state = (highest, totals, summed)
    running, totals, summed = state
    grid_result = jnp.transpose(summed / totals[..., None], (2, 0, 1, 3))
    grid_result = grid_result.reshape(row_count, grid_heads * HEAD).astype(jnp.bfloat16)
    local_heads = local_query_weight.shape[1] // HEAD
    local_groups = local_key_weight.shape[1] // HEAD
    local_size = local_heads // local_groups
    blocks = row_count // WINDOW
    local_queries = project(local_query_weight).reshape(
        blocks, WINDOW, local_groups, local_size, HEAD
    )
    pairs = jnp.stack(
        [
            project(local_key_weight).reshape(row_count, local_groups, HEAD),
            project(local_value_weight).reshape(row_count, local_groups, HEAD),
        ],
        axis=1,
    )
    widened = padded(pairs, (("sp", 0),), WINDOW)
    framed = widened.reshape(blocks + 2, WINDOW, 2, local_groups, HEAD)
    band = jnp.concatenate([framed[:-2], framed[1:-1], framed[2:]], axis=1)
    scores = (
        jnp.einsum(
            "nqhgd,nshd->hgnqs", local_queries, band[:, :, 0], preferred_element_type=jnp.float32
        )
        * score_scale
    )
    relative = jnp.arange(3 * WINDOW)[None, :] - WINDOW - jnp.arange(WINDOW)[:, None]
    key_pos = (
        offset + jnp.arange(blocks)[:, None] * WINDOW - WINDOW + jnp.arange(3 * WINDOW)[None, :]
    )
    valid = (jnp.abs(relative) <= WINDOW)[None] & ((key_pos >= 0) & (key_pos < total_rows))[
        :, None, :
    ]
    scores = jnp.where(valid, scores, -jnp.inf)
    sink = sink_logit.reshape(local_groups, local_size, 1, 1, 1)
    top = jnp.maximum(jnp.max(scores, axis=-1, keepdims=True), sink)
    lifted = jnp.exp(scores - top)
    weights = (lifted / (jnp.sum(lifted, axis=-1, keepdims=True) + jnp.exp(sink - top))).astype(
        jnp.bfloat16
    )
    local_result = jnp.einsum(
        "hgnqs,nshd->nqhgd", weights, band[:, :, 1], preferred_element_type=jnp.float32
    )
    local_result = local_result.astype(jnp.bfloat16).reshape(row_count, local_heads * HEAD)
    joined = lax.psum_scatter(
        jnp.concatenate(
            [
                jnp.dot(grid_result, grid_out_weight, preferred_element_type=jnp.float32),
                jnp.dot(local_result, local_out_weight, preferred_element_type=jnp.float32),
            ],
            axis=1,
        ).astype(jnp.bfloat16),
        "tp",
        scatter_dimension=0,
        tiled=True,
    ).astype(jnp.float32)
    merged = joined[:, :width] + joined[:, width:]
    return merged.astype(jnp.bfloat16)


def solution(mesh):
    in_specs = (
        P("sp", None),
        P(),
        P(None, "tp"),
        P(None, "tp"),
        P(None, "tp"),
        P(),
        P(),
        P(None, "tp"),
        P(None, "tp"),
        P(None, "tp"),
        P("tp"),
        P("tp", None),
        P("tp", None),
    )
    out_specs = P(("sp", "tp"), None)
    return jax.shard_map(shards, mesh=mesh, in_specs=in_specs, out_specs=out_specs, check_vma=False)
```

profile of v0, /device:TPU:1, one launch (start us, length us, event | category | flops | bytes accessed | tf_op | source)
XLA Modules:
  0.0 202.3 jit_solution(9195649055847436234)
XLA Ops:
  6.6 1.4 multiply_sine_fusion.1
  8.7 2.6 %fusion.6 = f32[768]{0:T(1024)S(1)} fusion(bf16[768,2048]{1,0:T(8,128)(2,1)} %param.13), kind=kLoop, calls=%fused_computation.9 | loop fusion | flops 4717824 | bytes 3148800 | tf_op jit(solution)/shard_map/reduce_sum | solution.py:30
  11.3 0.8 fusion.8
  12.4 1.2 multiply_reduce_fusion.1
  14.8 3.0 %convolution_convert_fusion.6 = bf16[768,128]{1,0:T(8,128)(2,1)S(1)} fusion(bf16[768,2048]{1,0:T(8,128)(2,1)} %copy-done.1, bf16[2048,128]{1,0:T(8,128)(2,1)S(1)} %copy-done.24), kind=kOutput, calls=%fused_computation.32 | convolution fusion | flops 402751488 | bytes 3866624 | tf_op jit(solution)/shard_map/dot_general | solution.py:79
  17.8 1.0 convolution_convert_fusion.5
  19.5 4.6 %collective-permute-start = (bf16[128,2,1,128]{3,0,2,1:T(8,128)(2,1)}, bf16[128,2,1,128]{3,0,2,1:T(8,128)(2,1)}, u32[]{:S(2)}, u32[]{:S(2)}) collective-permute-start(bf16[128,2,1,128]{3,0,2,1:T(8,128)(2,1)} %get-tuple-element.19), channel_id=1, source_target_pairs={{0,8},{8,16},{16,24},{24,32},{32,40},{40,48},{48,56},{56,64},{64,7... | collective-permute-start | bytes 196616 | tf_op jit(solution)/shard_map/ppermute | solution.py:20
  24.1 1.3 collective-permute-start.1
  25.4 1.9 convolution_convert_fusion.7
  27.4 0.9 copy.27
  28.3 0.9 copy.29
  29.3 3.0 %multiply_reduce_fusion = (f32[768,2]{0,1:T(2,128)S(1)}, bf16[768,256]{0,1:T(8,128)(2,1)S(1)}) fusion(bf16[768,2048]{1,0:T(8,128)(2,1)} %copy-done.1, bf16[2048,256]{1,0:T(8,128)(2,1)S(1)} %copy-done.23), kind=kOutput, calls=%fused_computation.51 | convolution fusion | flops 806091264 | bytes 4593664 | tf_op jit(solution)/shard_map/dot_general | solution.py:79
  32.8 1.9 slice_negate_fusion.1
  35.3 1.8 copy.28
  37.8 1.8 copy.30
  39.7 4.1 %convolution_convert_fusion.3 = bf16[768,256]{1,0:T(8,128)(2,1)} fusion(bf16[768,2048]{1,0:T(8,128)(2,1)} %copy-done.1, bf16[2048,256]{1,0:T(8,128)(2,1)} %param.20), kind=kOutput, calls=%fused_computation.24 | convolution fusion | flops 805502976 | bytes 4587520 | tf_op jit(solution)/shard_map/dot_general | solution.py:79
  44.0 1.6 fusion.37
  46.1 1.1 reshape.677
  47.2 1.2 pad_maximum_fusion.4
  48.4 1.2 pad_maximum_fusion.1
  50.9 0.9 fusion.14
  52.2 2.7 %convolution_convert_fusion = bf16[768,2048]{1,0:T(8,128)(2,1)} fusion(bf16[256,2048]{1,0:T(8,128)(2,1)S(1)} %copy-done, bf16[96,8,2,128]{3,2,1,0:T(2,128)(2,1)S(1)} %bitcast.134), kind=kOutput, calls=%fused_computation.13 | convolution fusion | flops 806879232 | bytes 4587520 | tf_op jit(solution)/shard_map/dot_general | solution.py:170
  54.9 11.1 %all-gather.4.cloned.1.call-done = bf16[12288,1,128]{0,2,1:T(8,128)(2,1)} async-done(((bf16[768,1,128]{0,2,1:T(8,128)(2,1)}), bf16[12288,1,128]{0,2,1:T(8,128)(2,1)}) %all-gather.4.cloned.1.call-update) | async-done | bytes 3145744 | tf_op jit(solution)/shard_map/all_gather | solution.py:106
  66.0 29.2 %bitcast_reduce_fusion = (f32[2,768]{1,0:T(2,128)S(1)}, f32[12288,768,2]{1,0,2:T(8,128)}) fusion(bf16[768,2,64]{2,0,1:T(8,128)(2,1)S(1)} %copy-done.10, bf16[768,2,64]{2,0,1:T(8,128)(2,1)S(1)} %copy-done.9, bf16[12288,1,128]{0,2,1:T(8,128)(2,1)} %all-gather.4.cloned.1.call-done), kind=kOutput, calls=%fused_computation.1 | convolution fusion | flops 4870371840 | bytes 79042560 | tf_op jit(solution)/shard_map/qhgd,shd->hgqs/dot_general | solution.py:103
  95.2 24.6 %fusion.1 = f32[2,768]{1,0:T(2,128)S(1)} fusion(f32[12288,768,2]{1,0,2:T(8,128)} %get-tuple-element.40, f32[2,768]{1,0:T(2,128)S(1)} %get-tuple-element.39), kind=kLoop, calls=%fused_computation.3 | loop fusion | flops 56621568 | bytes 75509760 | tf_op jit(solution)/shard_map/reduce_sum | solution.py:114
  119.9 27.1 %fusion.28 = bf16[2,768,128]{1,2,0:T(8,128)(2,1)S(1)} fusion(f32[12288,768,2]{1,0,2:T(8,128)} %get-tuple-element.40, f32[2,768]{1,0:T(2,128)S(1)} %get-tuple-element.39, bf16[12288,128]{0,1:T(8,128)(2,1)} %all-gather.6.cloned.1.call-done, f32[2,768]{1,0:T(2,128)S(1)} %get-tuple-element.24, f32[2,768]{1,0:T(2,128)S(1)} %get-tuple-element.23), kind=kOutput, calls=%fused_computation.37 | convolution fusion | flops 4889051136 | bytes 79054848 | tf_op jit(solution)/shard_map/hgqs,shd->hgqd/dot_general | solution.py:115
  147.0 1.0 convolution_convert_fusion.1
  148.0 0.9 copy-done.3
  148.9 3.4 %pad_maximum_fusion = bf16[768,4096]{1,0:T(8,128)(2,1)} fusion(bf16[768,2048]{1,0:T(8,128)(2,1)S(1)} %copy-done.3, bf16[768,2048]{1,0:T(8,128)(2,1)S(1)} %convolution_convert_fusion.1), kind=kLoop, calls=%fused_computation.12 | loop fusion | flops 12582912 | bytes 12582912 | tf_op jit(solution)/shard_map/concatenate | solution.py:167
  152.3 41.3 %reduce-scatter.2.cloned.1.call-done = bf16[96,4096]{1,0:T(8,128)(2,1)} async-done(((bf16[768,4096]{1,0:T(8,128)(2,1)}), bf16[96,4096]{1,0:T(8,128)(2,1)}) %reduce-scatter.2.cloned.1.call-update) | async-done | bytes 786448 | tf_op jit(solution)/shard_map/reduce_scatter | solution.py:166
  193.7 1.3 convert_element_type.118
  194.9 0.8 fusion.33
  (86 shorter events, 7.2 us)
Async XLA Ops:
  6.5 45.7 %copy-start = (bf16[256,2048]{1,0:T(8,128)(2,1)S(1)}, bf16[256,2048]{1,0:T(8,128)(2,1)}, u32[]{:S(2)}) copy-start(bf16[256,2048]{1,0:T(8,128)(2,1)} %param.25) | copy-start | bytes 3145732
  6.5 4.7 %copy-start.19 = (f32[2048]{0:T(1024)S(1)}, f32[2048]{0:T(1024)}, u32[]{:S(2)}) copy-start(f32[2048]{0:T(1024)} %param.14) | copy-start | bytes 24580
  6.5 59.5 %all-gather.4.cloned.1.call-start = ((), (), s32[]{:S(2)}) async-start(), calls=%async_computation.1 | async-start | bytes 3342336 | tf_op jit(solution)/shard_map/all_gather | solution.py:106
  6.6 4.7 %copy-start.4 = (bf16[768,2048]{1,0:T(8,128)(2,1)S(1)}, bf16[768,2048]{1,0:T(8,128)(2,1)}, u32[]{:S(2)}) copy-start(bf16[768,2048]{1,0:T(8,128)(2,1)} %param.13) | copy-start | bytes 9437188
  11.3 1.0 copy-start.16
  12.3 1.6 copy-start.1
  12.3 1.2 copy-start.22
  12.3 2.4 %copy-start.24 = (bf16[2048,128]{1,0:T(8,128)(2,1)S(1)}, bf16[2048,128]{1,0:T(8,128)(2,1)}, u32[]{:S(2)}) copy-start(bf16[2048,128]{1,0:T(8,128)(2,1)} %param.21) | copy-start | bytes 1572868
  14.0 3.8 %copy-start.25 = (bf16[2048,128]{1,0:T(8,128)(2,1)S(1)}, bf16[2048,128]{1,0:T(8,128)(2,1)}, u32[]{:S(2)}) copy-start(bf16[2048,128]{1,0:T(8,128)(2,1)} %param.22) | copy-start | bytes 1572868
  14.7 105.2 %all-gather.6.cloned.1.call-start = ((), (), s32[]{:S(2)}) async-start(), calls=%async_computation.3 | async-start | bytes 3342336 | tf_op jit(solution)/shard_map/all_gather | solution.py:118
  14.7 3.0 %copy-start.2 = (bf16[768,2048]{1,0:T(8,128)(2,1)S(1)}, bf16[768,2048]{1,0:T(8,128)(2,1)}, u32[]{:S(2)}) copy-start(bf16[768,2048]{1,0:T(8,128)(2,1)} %copy-done.1) | copy-start | bytes 9437188
  17.8 1.0 copy-start.7
  17.8 7.6 %copy-start.17 = (bf16[2048,128]{1,0:T(8,128)(2,1)S(1)}, bf16[2048,128]{1,0:T(8,128)(2,1)}, u32[]{:S(2)}) copy-start(bf16[2048,128]{1,0:T(8,128)(2,1)} %param.17) | copy-start | bytes 1572868
  18.8 0.7 copy-start.8
  18.8 10.5 %copy-start.23 = (bf16[2048,256]{1,0:T(8,128)(2,1)S(1)}, bf16[2048,256]{1,0:T(8,128)(2,1)}, u32[]{:S(2)}) copy-start(bf16[2048,256]{1,0:T(8,128)(2,1)} %param.15) | copy-start | bytes 3145732
  19.5 27.6 %collective-permute-start = (bf16[128,2,1,128]{3,0,2,1:T(8,128)(2,1)}, bf16[128,2,1,128]{3,0,2,1:T(8,128)(2,1)}, u32[]{:S(2)}, u32[]{:S(2)}) collective-permute-start(bf16[128,2,1,128]{3,0,2,1:T(8,128)(2,1)} %get-tuple-element.19), channel_id=1, source_target_pairs={{0,8},{8,16},{16,24},{24,32},{32,40},{40,48},{48,56},{56,64},{64,7... | collective-permute-start | bytes 196616 | tf_op jit(solution)/shard_map/ppermute | solution.py:20
  24.1 23.0 %collective-permute-start.1 = (bf16[128,2,1,128]{3,0,2,1:T(8,128)(2,1)}, bf16[128,2,1,128]{3,0,2,1:T(8,128)(2,1)}, u32[]{:S(2)}, u32[]{:S(2)}) collective-permute-start(bf16[128,2,1,128]{3,0,2,1:T(8,128)(2,1)} %get-tuple-element.20), channel_id=1, source_target_pairs={{8,0},{16,8},{24,16},{32,24},{40,32},{48,40},{56,48},{64,56},{72,6... | collective-permute-start | bytes 196616 | tf_op jit(solution)/shard_map/ppermute | solution.py:23
  27.3 166.3 %reduce-scatter.2.cloned.1.call-start = ((), (), s32[]{:S(2)}) async-start(), calls=%async_computation.2 | async-start | bytes 7077888 | tf_op jit(solution)/shard_map/reduce_scatter | solution.py:166
  29.3 3.2 %copy-start.21 = (f32[128]{0:T(128)S(1)}, f32[128]{0:T(128)}, u32[]{:S(2)}) copy-start(f32[128]{0:T(128)} %param.18) | copy-start | bytes 1540
  32.7 1.9 copy-start.18
  39.7 4.3 %copy-start.5 = (f32[768,2,32]{2,0,1:T(8,128)S(1)}, f32[768,2,32]{2,0,1:T(8,128)}, u32[]{:S(2)}) copy-start(f32[768,2,32]{2,0,1:T(8,128)} %get-tuple-element.9) | copy-start | bytes 589828
  39.7 4.3 %copy-start.6 = (f32[768,2,32]{2,0,1:T(8,128)S(1)}, f32[768,2,32]{2,0,1:T(8,128)}, u32[]{:S(2)}) copy-start(f32[768,2,32]{2,0,1:T(8,128)} %get-tuple-element.10) | copy-start | bytes 589828
  39.7 4.3 %copy-start.11 = (f32[768,64]{1,0:T(8,128)S(1)}, f32[768,64]{1,0:T(8,128)}, u32[]{:S(2)}) copy-start(f32[768,64]{1,0:T(8,128)} %copy.27) | copy-start | bytes 589828
  39.7 4.3 %copy-start.12 = (f32[768,64]{1,0:T(8,128)S(1)}, f32[768,64]{1,0:T(8,128)}, u32[]{:S(2)}) copy-start(f32[768,64]{1,0:T(8,128)} %copy.29) | copy-start | bytes 589828
  39.7 4.3 %copy-start.13 = (f32[768,64]{1,0:T(8,128)S(1)}, f32[768,64]{1,0:T(8,128)}, u32[]{:S(2)}) copy-start(f32[768,64]{1,0:T(8,128)} %copy.28) | copy-start | bytes 589828
  39.7 4.3 %copy-start.14 = (f32[768,64]{1,0:T(8,128)S(1)}, f32[768,64]{1,0:T(8,128)}, u32[]{:S(2)}) copy-start(f32[768,64]{1,0:T(8,128)} %copy.30) | copy-start | bytes 589828
  48.4 1.8 copy-start.20
  52.2 13.8 %copy-start.9 = (bf16[768,2,64]{2,0,1:T(8,128)(2,1)S(1)}, bf16[768,2,64]{2,0,1:T(8,128)(2,1)}, u32[]{:S(2)}) copy-start(bf16[768,2,64]{2,0,1:T(8,128)(2,1)} %get-tuple-element.5) | copy-start | bytes 589828
  52.2 13.8 %copy-start.10 = (bf16[768,2,64]{2,0,1:T(8,128)(2,1)S(1)}, bf16[768,2,64]{2,0,1:T(8,128)(2,1)}, u32[]{:S(2)}) copy-start(bf16[768,2,64]{2,0,1:T(8,128)(2,1)} %get-tuple-element.6) | copy-start | bytes 589828
  119.9 27.1 %copy-start.15 = (bf16[256,2048]{1,0:T(8,128)(2,1)S(1)}, bf16[256,2048]{1,0:T(8,128)(2,1)}, u32[]{:S(2)}) copy-start(bf16[256,2048]{1,0:T(8,128)(2,1)} %param.24) | copy-start | bytes 3145732
  147.0 1.9 copy-start.3
Sparse Core Ops, SparseCore 0:
  14.8 51.1 all-gather.3
  68.2 46.9 all-gather.5
  152.5 41.1 reduce-scatter.1
where the time goes:
time: 203 us; the launch traced here: 202 us
  matrix products  75.4 us (37%)
  waiting for transfers between devices  52.5 us (26%)
  other arithmetic  46.2 us (23%)
  between operations  13.6 us (7%)
  local copies, waits for them, and re-layouts  8.64 us (4%)
  starting transfers between devices  5.99 us (3%)
    reduce_scatter x1, waiting for transfers between devices, shards(): lax.psum_scatter(jnp.concatenate([jnp.dot(grid_result, grid_out_weight, p...  41.3 us
    dot_general x1, matrix products, shards(): jnp.einsum('qhgd,shd->hgqs', queries, lax.all_gather(keys, 'sp', axis=0,...  29.2 us
    dot_general x1, matrix products, shards(): jnp.einsum('hgqs,shd->hgqd', weights.astype(jnp.bfloat16), lax.all_gather...  27.1 us
    reduce_sum x1, other arithmetic, shards(): totals = totals * factor + jnp.sum(weights, axis=-1)  24.6 us
    dot_general x6, matrix products, project(): jnp.dot(normed, weight, preferred_element_type=jnp.float32)  14.1 us
    all_gather x1, waiting for transfers between devices, shards(): lax.all_gather(keys, 'sp', axis=0, tiled=True)  11.1 us
    mul x4, local copies, waits for them, and re-layouts, half_turn(): return part * cosine + turned * sine  5.54 us
    ppermute x1, starting transfers between devices, padded(): lax.ppermute(lax.slice_in_dim(block, block.shape[dim] - width, None, axis...  4.62 us
  transfers between devices with their start and end apart: 5, of which 2 were waited for; matrix products, arithmetic and copies ran while one was open for 43% of the time, Pallas kernels for 0%

commit v1 on v0

v1 whole, which is shorter than its diff:
```python
import functools
import math

import jax
import jax.numpy as jnp
import numpy as np
from jax import lax
from jax.experimental import pallas as pl
from jax.experimental.pallas import tpu as pltpu
from jax.sharding import PartitionSpec as P

D = 2048
HEAD = 128
WINDOW = 128
GRID_W = 64
ROWS = 768
EPSILON = 1e-06
ROPE_BASE = 10000.0
LOG2E = math.log2(math.e)
SCORE = HEAD ** (-0.5) * LOG2E
NSP = 16
SIDE = 4
BLOCKS = 4
PART = 48
TILES = 5
EARLY = 40
BF = jnp.bfloat16
F32 = jnp.float32
MESH = pl.DeviceIdType.MESH


def dot(a, b):
    return jnp.dot(a, b, preferred_element_type=F32)


def rope_tables():
    half = HEAD // 2
    inverse = ROPE_BASE ** (-np.arange(0, half, 2, dtype=np.float64) / half)
    sign = np.concatenate([-np.ones(half // 2), np.ones(half // 2)])

    def table(count):
        angle = np.arange(count)[:, None] * np.concatenate([inverse, inverse])
        return np.cos(angle), np.sin(angle) * sign

    rows = np.zeros((2, NSP, 16, HEAD), np.float32)
    cosine, sine = table(NSP * ROWS // GRID_W)
    per = ROWS // GRID_W
    rows[0, :, :per, :half] = cosine.reshape(NSP, per, half)
    rows[1, :, :per, :half] = sine.reshape(NSP, per, half)
    cols = np.zeros((2, GRID_W, HEAD), np.float32)
    cosine, sine = table(GRID_W)
    cols[0, :, half:] = cosine
    cols[1, :, half:] = sine
    return np.ascontiguousarray(rows.transpose(1, 0, 2, 3)), cols


def kernel(
    tokens,
    gain,
    wq,
    wk,
    wv,
    gain_q,
    gain_k,
    lwq,
    lwk,
    lwv,
    sink,
    wog,
    wol,
    row_table,
    col_table,
    out,
    xs,
    xn,
    wg,
    wl,
    wo,
    rows_tab,
    qr,
    qs,
    qp,
    kall,
    vall,
    m,
    l,
    o,
    s0,
    s1,
    lq,
    lk,
    lv,
    lo,
    osend,
    orecv,
    keep,
    dsend,
    drecv,
    x0,
    x12,
    ra,
    r1,
    in_sem,
    kv_s,
    kv_r,
    q_s,
    q_r,
    h_s,
    h_r,
    o_s,
    o_r,
    d_s,
    d_r,
    x_s,
    x_r,
):
    sp = lax.axis_index("sp")
    tp = lax.axis_index("tp")
    core = lax.rem(tp, 2)
    x = tp // 2
    z = sp // SIDE
    y = lax.rem(sp, SIDE)

    def along_z(d):
        return lax.rem(z + d, SIDE) * SIDE + y

    def along_y(d):
        return z * SIDE + lax.rem(y + d, SIDE)

    def q_peer(d):
        return {"sp": along_z(d) * (1 - core) + along_y(d) * core, "tp": tp}

    def kv_peer(d):
        return {"sp": along_z(d) * core + along_y(d) * (1 - core), "tp": tp}

    def sp_peer(d):
        return {"sp": lax.rem(sp + d, NSP), "tp": tp}

    def x_peer(d):
        return {"sp": sp, "tp": lax.rem(x + d, SIDE) * 2 + core}

    partner = {"sp": sp, "tp": x * 2 + 1 - core}

    def remote(src, dst, send, recv, peer):
        return pltpu.make_async_remote_copy(
            src_ref=src, dst_ref=dst, send_sem=send, recv_sem=recv, device_id=peer, device_id_type=MESH
        )

    def local(src, dst, i):
        return pltpu.make_async_copy(src, dst, in_sem.at[i])

    third = ROWS // 3
    loads = [
        local(tokens.at[pl.ds(0, third)], xs.at[pl.ds(0, third)], 0),
        local(wk, wg.at[:, pl.ds(256, 128)], 1),
        local(wv, wg.at[:, pl.ds(384, 128)], 2),
        local(wq, wg.at[:, pl.ds(0, 256)], 3),
        local(row_table.at[sp], rows_tab, 4),
        local(tokens.at[pl.ds(third, third)], xs.at[pl.ds(third, third)], 5),
        local(tokens.at[pl.ds(2 * third, third)], xs.at[pl.ds(2 * third, third)], 6),
        local(lwq, wl.at[:, pl.ds(0, 256)], 7),
        local(lwk, wl.at[:, pl.ds(256, 128)], 8),
        local(lwv, wl.at[:, pl.ds(384, 128)], 9),
        local(wog, wo.at[pl.ds(0, 256)], 10),
        local(wol, wo.at[pl.ds(256, 256)], 11),
    ]
    for load in loads:
        load.start()

    barrier = pltpu.get_barrier_semaphore()
    peers = [q_peer(1), q_peer(2), q_peer(3), kv_peer(1), kv_peer(3), sp_peer(1), sp_peer(NSP - 1)]
    peers += [x_peer(1), x_peer(3), partner]
    for peer in peers:
        pl.semaphore_signal(barrier, inc=1, device_id=peer, device_id_type=MESH)

    m[...] = jnp.full_like(m, -1e30)
    l[...] = jnp.zeros_like(l)
    o[...] = jnp.zeros_like(o)
    vall[:, pl.ds(HEAD, 16), :] = jnp.ones((SIDE, 16, ROWS), BF)

    lane = lax.broadcasted_iota(jnp.int32, (third, HEAD), 1)
    first_half = lax.rem(lane, 64) < 32

    def norm(r):
        block = xs[pl.ds(r * third, third), :].astype(F32)
        mean = jnp.mean(block * block, axis=-1, keepdims=True)
        xn[pl.ds(r * third, third), :] = (block * lax.rsqrt(mean + EPSILON) * gain[...]).astype(BF)

    def rope(u, gain_row, r):
        mean = jnp.mean(u * u, axis=-1, keepdims=True)
        u = u * lax.rsqrt(mean + EPSILON) * gain_row
        swapped = jnp.where(first_half, pltpu.roll(u, HEAD - 32, 1), pltpu.roll(u, 32, 1))
        per = third // GRID_W

        def table(which):
            return jnp.concatenate(
                [col_table[which] + rows_tab[which, pl.ds(r * per + i, 1), :] for i in range(per)], axis=0
            )

        return (u * table(0) + swapped * table(1)).astype(BF)

    def project_grid(r):
        rows = pl.ds(r * third, third)
        p = dot(xn[rows, :], wg[...])
        kall[0, rows, :] = rope(p[:, 256:384], gain_k[...], r)
        vall[0, pl.ds(0, HEAD), rows] = p[:, 384:512].T.astype(BF)
        scaled = gain_q[...] * SCORE
        qr[0, rows, :] = rope(p[:, 0:128], scaled, r)
        qr[1, rows, :] = rope(p[:, 128:256], scaled, r)

    loads[0].wait()
    norm(0)
    for i in (1, 2, 3, 4, 5):
        loads[i].wait()
    norm(1)
    project_grid(0)
    loads[6].wait()
    norm(2)
    project_grid(1)
    project_grid(2)

    pl.semaphore_wait(barrier, len(peers))
    value_rows = pl.ds(0, HEAD)
    sends = []

    def send(*args):
        copy = remote(*args)
        copy.start()
        sends.append(copy)

    def k_copy(slot_from, slot_to, s, d):
        return (kall.at[slot_from], kall.at[slot_to], kv_s.at[s], kv_r.at[0, slot_to], kv_peer(d))

    def v_copy(slot_from, slot_to, s, d):
        return (
            vall.at[slot_from, value_rows],
            vall.at[slot_to, value_rows],
            kv_s.at[s],
            kv_r.at[1, slot_to],
            kv_peer(d),
        )

    k_up, k_down = k_copy(0, 3, 0, 1), k_copy(0, 1, 1, 3)
    v_up, v_down = v_copy(0, 3, 2, 1), v_copy(0, 1, 3, 3)
    for args in (k_up, v_down, k_down, v_up):
        send(*args)
    k_relay, v_relay = k_copy(3, 2, 4, 1), v_copy(1, 2, 5, 3)

    ahead, behind, across = (lax.rem(x + d, SIDE) * 192 for d in (1, 3, 2))
    own = x * 192
    starts = (
        (across, across + 48, across + 96, across + 144),
        (ahead, behind, ahead + 96, behind + 96),
        (ahead + 48, behind + 48, ahead + 144, behind + 144),
        (own, own + 48, own + 96, own + 144),
    )

    def gather(ref, k):
        return jnp.concatenate([ref[pl.ds(pl.multiple_of(s, 16), PART), :] for s in starts[k]], axis=0)

    for k in range(BLOCKS):
        one, two = gather(qr.at[0], k), gather(qr.at[1], k)
        pieces = (one[:128], jnp.concatenate([one[128:], two[:64]], axis=0), two[64:])
        for i, piece in enumerate(pieces):
            turned = piece.astype(F32).T.astype(BF)
            qs[k, i] = turned
            qp[k * 10 + 9 if i == 2 else EARLY + 2 * k + i] = turned

    place = {2: 0, 1: 3, 3: 6}

    def q_copy(source, k, slot, s, d):
        return (source, qp.at[pl.ds(k * 10 + place[slot], 3)], q_s.at[k, s], q_r.at[k, slot], q_peer(d))

    def send_queries(k):
        send(*q_copy(qs.at[k], k, 3, 0, 1))
        send(*q_copy(qs.at[k], k, 1, 1, 3))

    def relay_queries(k):
        arrived = 3 if k % 2 == 0 else 1
        wait_queries(k, arrived)
        send(*q_copy(qp.at[pl.ds(k * 10 + place[arrived], 3)], k, 2, 2, 4 - arrived))

    def wait_queries(k, slot):
        args = q_copy(qs.at[k], k, slot, 0, 1)
        remote(*args).wait_recv()

    for i in (7, 8, 9):
        loads[i].wait()
    for r in range(3):
        rows = pl.ds(r * third, third)
        p = dot(xn[rows, :], wl[...])
        lq[rows, :] = (p[:, 0:256] * SCORE).astype(BF)
        lk[pl.ds(WINDOW + r * third, third), :] = p[:, 256:384].astype(BF)
        lv[pl.ds(WINDOW + r * third, third), :] = p[:, 384:512].astype(BF)

    def halo(ref, i, low):
        source, target, d = (ROWS, 0, 1) if low else (WINDOW, ROWS + WINDOW, NSP - 1)
        j = 2 * i + (0 if low else 1)
        return (
            ref.at[pl.ds(source, WINDOW)],
            ref.at[pl.ds(target, WINDOW)],
            h_s.at[j],
            h_r.at[j],
            sp_peer(d),
        )

    halos = [halo(ref, i, low) for i, ref in enumerate((lk, lv)) for low in (True, False)]
    for args in halos:
        send(*args)

    def attend(base, tiles, slots, count):
        units = tiles * count // 2

        def where(u):
            halves = []
            for h in range(2):
                index = 2 * u + h
                halves.append((slots(index // tiles), base + 2 * lax.rem(index, tiles)))
            return halves

        def scores(u, ref):
            tops = []
            for h, (t, g) in enumerate(where(u)):
                queries = jnp.concatenate([qp[g], qp[g + 1]], axis=1)
                s = dot(kall[t], queries)
                ref[h] = s
                tops.append(jnp.max(s, axis=0, keepdims=True))
            return tops

        def weigh(u, ref, tops):
            for h, (t, g) in enumerate(where(u)):
                before = jnp.concatenate([m[g], m[g + 1]], axis=1)
                top = jnp.maximum(before, tops[h])
                factor = jnp.exp2(before - top)
                weights = jnp.exp2(ref[h] - top).astype(BF)
                result = dot(vall[t], weights)
                for i in range(2):
                    part = slice(i * 128, i * 128 + 128)
                    m[g + i] = top[:, part]
                    l[g + i] = l[g + i] * factor[:, part] + result[HEAD : HEAD + 1, part]
                    o[g + i] = o[g + i] * factor[:, part] + result[:HEAD, part]

        tops = scores(0, s0)

        def body(i, tops):
            u = 2 * i
            later = scores(u + 1, s1)
            weigh(u, s0, tops)
            tops = scores(jnp.minimum(u + 2, units - 1), s0)
            weigh(u + 1, s1, later)
            return tops

        lax.fori_loop(0, units // 2, body, tops)

    attend(EARLY, 4, lambda i: i * 0, 1)

    for args in halos:
        remote(*args).wait_recv()
    wide = 3 * WINDOW
    row = lax.rem(lax.broadcasted_iota(jnp.int32, (2 * WINDOW, wide), 0), WINDOW)
    col = lax.broadcasted_iota(jnp.int32, (2 * WINDOW, wide), 1)
    near = (col >= row) & (col <= row + 2 * WINDOW)
    sink_rows = jnp.concatenate(
        [jnp.full((WINDOW, 1), sink[0] * LOG2E, F32), jnp.full((WINDOW, 1), sink[1] * LOG2E, F32)], axis=0
    )
    blocks = ROWS // WINDOW

    def banded(n, carry):
        at = pl.multiple_of(n * WINDOW, WINDOW)
        rows = lq[pl.ds(at, WINDOW), :]
        queries = jnp.concatenate([rows[:, :HEAD], rows[:, HEAD:]], axis=0)
        keys = lk[pl.ds(at, wide), :]
        s = lax.dot_general(queries, keys, (((1,), (1,)), ((), ())), preferred_element_type=F32)
        block = sp * blocks + n
        low = jnp.where(block == 0, WINDOW, 0)
        high = jnp.where(block == NSP * blocks - 1, 2 * WINDOW, wide)
        s = jnp.where(near & (col >= low) & (col < high), s, -1e30)
        top = jnp.maximum(jnp.max(s, axis=1, keepdims=True), sink_rows)
        lifted = jnp.exp2(s - top)
        total = jnp.sum(lifted, axis=1, keepdims=True) + jnp.exp2(sink_rows - top)
        result = dot(lifted.astype(BF), lv[pl.ds(at, wide), :]) / total
        lo[pl.ds(at, WINDOW), :] = jnp.concatenate([result[:WINDOW], result[WINDOW:]], axis=1).astype(BF)
        return carry

    lax.fori_loop(0, blocks, banded, 0)

    remote(*k_up).wait_recv()
    send(*k_relay)
    remote(*v_down).wait_recv()
    send(*v_relay)
    for k in range(BLOCKS):
        send_queries(k)
    remote(*k_down).wait_recv()
    remote(*v_up).wait_recv()
    attend(EARLY, 4, lambda i: 1 + 2 * i, 2)
    relay_queries(0)
    remote(*k_relay).wait_recv()
    remote(*v_relay).wait_recv()
    attend(EARLY, 4, lambda i: i * 0 + 2, 1)
    relay_queries(1)

    def packed(g):
        total = l[g]
        level = m[g] + jnp.log2(total)
        high = level.astype(BF)
        rest = level - high.astype(F32)
        mid = rest.astype(BF)
        low = (rest - mid.astype(F32)).astype(BF)
        tail = jnp.concatenate([high, mid, low, jnp.zeros((13, HEAD), BF)], axis=0)
        return jnp.concatenate([(o[g] / total).astype(BF), tail], axis=0)

    def o_copy(k, s):
        return (osend.at[k, s], orecv.at[k, 4 - s], o_s.at[k, s], o_r.at[k, 4 - s], q_peer(s))

    def send_results(k):
        for s in (2, 1, 3):
            for i in range(3):
                osend[k, s, i] = packed(k * 10 + place[s] + i)
            send(*o_copy(k, s))

    def merge(k):
        for s in (1, 3, 2):
            remote(*o_copy(k, s)).wait_recv()
        merged = []
        for i in range(3):
            g = k * 10 + 9 if i == 2 else EARLY + 2 * k + i
            levels = []
            for s in (1, 2, 3):
                rows = orecv[k, s, i, pl.ds(HEAD, 16), :].astype(F32)
                levels.append(rows[0:1] + rows[1:2] + rows[2:3])
            total = l[g]
            mine = m[g] + jnp.log2(total)
            top = functools.reduce(jnp.maximum, levels, mine)
            share = jnp.exp2(mine - top)
            shares = [jnp.exp2(level - top) for level in levels]
            whole = share + shares[0] + shares[1] + shares[2]
            acc = o[g] * (share / (total * whole))
            for s in (1, 2, 3):
                acc += orecv[k, s, i, value_rows, :].astype(F32) * (shares[s - 1] / whole)
            merged.append(acc.T.astype(BF))
        one = jnp.concatenate([merged[0], merged[1][:64]], axis=0)
        two = jnp.concatenate([merged[1][64:], merged[2]], axis=0)
        features = jnp.concatenate([one, two, gather(lo, k)], axis=1)
        for c in range(2):
            keep[k, c] = dot(features[c * 96 : c * 96 + 96], wo[...])
        dsend[k] = keep[k, 1 - core].astype(BF)
        send(*d_copy(k))

    def d_copy(k):
        return (dsend.at[k], drecv.at[k], d_s.at[k], d_r.at[k], partner)

    half = D // 2

    def x_copy(i):
        if i < 2:
            return (x0.at[i], ra.at[i], x_s.at[i], x_r.at[i], x_peer(1 if i == 0 else 3))
        k, side = divmod(i - 2, 2)
        return (x12.at[k, side], r1.at[k, side], x_s.at[i], x_r.at[i], x_peer(1 if side == 0 else 3))

    def summed(k):
        remote(*d_copy(k)).wait_recv()
        return keep[k, core] + drecv[k].astype(F32)

    def scatter(k):
        total = summed(k)
        if k == 0:
            for i in range(2):
                x0[i] = total[:, i * half : i * half + half].astype(BF)
                send(*x_copy(i))
        elif k < 3:
            if k == 1:
                for i in range(2):
                    remote(*x_copy(i)).wait_recv()
            for side in range(2):
                mine = total[side * PART : side * PART + PART]
                passing = ra[side, pl.ds((k - 1) * PART, PART), :].astype(F32)
                if side == 0:
                    mine = jnp.concatenate([mine[:, :half] + passing, mine[:, half:]], axis=1)
                else:
                    mine = jnp.concatenate([mine[:, :half], mine[:, half:] + passing], axis=1)
                x12[k - 1, side] = mine.astype(BF)
                send(*x_copy(2 * k + side))
        else:
            for i in range(2, 6):
                remote(*x_copy(i)).wait_recv()
            for part in range(2):
                rows = slice(part * PART, part * PART + PART)
                both = r1[part, 0].astype(F32) + r1[part, 1].astype(F32)
                out[pl.ds(part * PART, PART), :] = (total[rows] + both).astype(BF)

    for i in (10, 11):
        loads[i].wait()
    for k in range(BLOCKS):
        if k == 0:
            wait_queries(0, 1)
        else:
            wait_queries(k, 1 if k % 2 == 0 else 3)
        wait_queries(k, 2)
        attend(k * 10, TILES, lambda i: i, SIDE)
        send_results(k)
        if k < 2:
            relay_queries(k + 2)
        if k > 0:
            merge(k - 1)
            scatter(k - 1)
    merge(3)
    scatter(3)
    for copy in sends:
        copy.wait_send()


def shards(
    tokens,
    norm_gain,
    grid_query_weight,
    grid_key_weight,
    grid_value_weight,
    grid_query_gain,
    grid_key_gain,
    local_query_weight,
    local_key_weight,
    local_value_weight,
    sink_logit,
    grid_out_weight,
    local_out_weight,
):
    row_table, col_table = rope_tables()
    hbm = pl.BlockSpec(memory_space=pl.ANY)
    vmem = pl.BlockSpec(memory_space=pltpu.VMEM)
    smem = pl.BlockSpec(memory_space=pltpu.SMEM)
    dma = pltpu.SemaphoreType.DMA
    return pl.pallas_call(
        kernel,
        out_shape=jax.ShapeDtypeStruct((96, D), BF),
        in_specs=[hbm, vmem, hbm, hbm, hbm, vmem, vmem, hbm, hbm, hbm, smem, hbm, hbm, hbm, vmem],
        out_specs=vmem,
        scratch_shapes=[
            pltpu.VMEM((ROWS, D), BF),
            pltpu.VMEM((ROWS, D), BF),
            pltpu.VMEM((D, 512), BF),
            pltpu.VMEM((D, 512), BF),
            pltpu.VMEM((512, D), BF),
            pltpu.VMEM((2, 16, HEAD), F32),
            pltpu.VMEM((2, ROWS, HEAD), BF),
            pltpu.VMEM((BLOCKS, 3, HEAD, HEAD), BF),
            pltpu.VMEM((48, HEAD, HEAD), BF),
            pltpu.VMEM((SIDE, ROWS, HEAD), BF),
            pltpu.VMEM((SIDE, HEAD + 16, ROWS), BF),
            pltpu.VMEM((48, 1, HEAD), F32),
            pltpu.VMEM((48, 1, HEAD), F32),
            pltpu.VMEM((48, HEAD, HEAD), F32),
            pltpu.VMEM((2, ROWS, 256), F32),
            pltpu.VMEM((2, ROWS, 256), F32),
            pltpu.VMEM((ROWS, 256), BF),
            pltpu.VMEM((ROWS + 2 * WINDOW, HEAD), BF),
            pltpu.VMEM((ROWS + 2 * WINDOW, HEAD), BF),
            pltpu.VMEM((ROWS, 256), BF),
            pltpu.VMEM((BLOCKS, 4, 3, HEAD + 16, HEAD), BF),
            pltpu.VMEM((BLOCKS, 4, 3, HEAD + 16, HEAD), BF),
            pltpu.VMEM((BLOCKS, 2, 96, D), F32),
            pltpu.VMEM((BLOCKS, 96, D), BF),
            pltpu.VMEM((BLOCKS, 96, D), BF),
            pltpu.VMEM((2, 96, D // 2), BF),
            pltpu.VMEM((2, 2, PART, D), BF),
            pltpu.VMEM((2, 96, D // 2), BF),
            pltpu.VMEM((2, 2, PART, D), BF),
            dma((12,)),
            dma((6,)),
            dma((2, 4)),
            dma((BLOCKS, 3)),
            dma((BLOCKS, 4)),
            dma((4,)),
            dma((4,)),
            dma((BLOCKS, 4)),
            dma((BLOCKS, 4)),
            dma((BLOCKS,)),
            dma((BLOCKS,)),
            dma((6,)),
            dma((6,)),
        ],
        compiler_params=pltpu.CompilerParams(
            collective_id=0, has_side_effects=True, vmem_limit_bytes=60 * 2**20
        ),
    )(
        tokens,
        norm_gain.reshape(1, D),
        grid_query_weight,
        grid_key_weight,
        grid_value_weight,
        grid_query_gain.reshape(1, HEAD),
        grid_key_gain.reshape(1, HEAD),
        local_query_weight,
        local_key_weight,
        local_value_weight,
        sink_logit,
        grid_out_weight,
        local_out_weight,
        jnp.asarray(row_table),
        jnp.asarray(col_table),
    )


def solution(mesh):
    in_specs = (
        P("sp", None),
        P(),
        P(None, "tp"),
        P(None, "tp"),
        P(None, "tp"),
        P(),
        P(),
        P(None, "tp"),
        P(None, "tp"),
        P(None, "tp"),
        P("tp"),
        P("tp", None),
        P("tp", None),
    )
    out_specs = P(("sp", "tp"), None)
    return jax.shard_map(shards, mesh=mesh, in_specs=in_specs, out_specs=out_specs, check_vma=False)
```

time: 203 us -> 70.1 us (0.35)
  matrix products: 75.4 us -> 0 us
  Pallas kernels: 0 us -> 68.1 us
  waiting for transfers between devices: 52.5 us -> 0 us
  other arithmetic: 46.2 us -> 0 us
  between operations: 13.6 us -> 0.01 us
  local copies, waits for them, and re-layouts: 8.64 us -> 1.77 us
  starting transfers between devices: 5.99 us -> 0 us
    dot_general x12 -> x0, matrix products: 75.4 us -> none  [the longest x1 29.2 us: shards(): jnp.einsum('qhgd,shd->hgqs', queries, lax.all_gather(keys, 'sp', axis=0,...]
    pallas_call x0 -> x1, Pallas kernels: none -> 68.1 us  [shards(): pl.pallas_call(kernel, out_shape=jax.ShapeDtypeStruct((96, D), BF), in_sp...]
    reduce_scatter x1 -> x0, waiting for transfers between devices: 41.3 us -> none  [shards(): lax.psum_scatter(jnp.concatenate([jnp.dot(grid_result, grid_out_weight, p...]
    reduce_sum x3 -> x0, other arithmetic: 27.8 us -> none  [the longest x1 24.6 us: shards(): totals = totals * factor + jnp.sum(weights, axis=-1)]
    all_gather x2 -> x0, waiting for transfers between devices: 11.1 us -> none  [the longest x1 11.1 us: shards(): lax.all_gather(keys, 'sp', axis=0, tiled=True)]
    concatenate x5 -> x0, other arithmetic: 7.33 us -> none  [the longest x1 3.45 us: shards(): jnp.concatenate([jnp.dot(grid_result, grid_out_weight, preferred_element_...]
    ppermute x2 -> x0, starting transfers between devices: 5.9 us -> none  [the longest x1 4.62 us: padded(): lax.ppermute(lax.slice_in_dim(block, block.shape[dim] - width, None, axis...]
    mul x4 -> x0, local copies, waits for them, and re-layouts: 5.54 us -> none  [half_turn(): return part * cosine + turned * sine]
  transfers between devices with their start and end apart: 5 -> 0, of which waited for: 2 -> 0; matrix products, arithmetic and copies ran while one was open for 43% -> 0% of each run, Pallas kernels for 0% -> 0%
where the time goes in v1:
time: 70.1 us; the launch traced here: 69.9 us
  Pallas kernels  68.1 us (97%)
  local copies, waits for them, and re-layouts  1.77 us (3%)
    pallas_call x1, Pallas kernels, shards(): pl.pallas_call(kernel, out_shape=jax.ShapeDtypeStruct((96, D), BF), in_sp...  68.1 us
    unnamed x1, local copies, waits for them, and re-layouts  1.77 us

profile of v1, /device:TPU:1, one launch (start us, length us, event | category | flops | bytes accessed | tf_op | source)
XLA Modules:
  0.0 69.9 jit_solution(2748283906253684295)
XLA Ops:
  0.0 68.1 %shard_map.145 = bf16[96,2048]{1,0:T(8,128)(2,1)} custom-call(bf16[768,2048]{1,0:T(8,128)(2,1)} %tokens.1, f32[1,2048]{1,0:T(1,128)} %bitcast.3, bf16[2048,256]{1,0:T(8,128)(2,1)} %wq.1, bf16[2048,128]{1,0:T(8,128)(2,1)} %wk.1, bf16[2048,128]{1,0:T(8,128)(2,1)} %wv.1, f32[1,128]{1,0:T(1,128)} %bitcast.4, f32[1,128]{1,0:T(1,128)} %bitcast.5, ...), custom_call_target="tpu_custom_call" | custom-call | tf_op jit(solution)/shard_map/pallas_call | solution.py:532
  68.1 1.8 %copy.17 = bf16[96,2048]{1,0:T(8,128)(2,1)} copy(bf16[96,2048]{1,0:T(8,128)(2,1)} %shard_map.145) | data formatting | bytes 786432

commit v2 on v1

--- a/solution.py
+++ b/solution.py
@@ -21,8 +21,8 @@
 NSP = 16
 SIDE = 4
 BLOCKS = 4
+CHUNK = 32
 PART = 48
-TILES = 5
 EARLY = 40
 BF = jnp.bfloat16
 F32 = jnp.float32
@@ -73,7 +73,8 @@
     out,
     xs,
     xn,
-    wg,
+    wkv,
+    wqg,
     wl,
     wo,
     rows_tab,
@@ -152,12 +153,12 @@
     third = ROWS // 3
     loads = [
         local(tokens.at[pl.ds(0, third)], xs.at[pl.ds(0, third)], 0),
-        local(wk, wg.at[:, pl.ds(256, 128)], 1),
-        local(wv, wg.at[:, pl.ds(384, 128)], 2),
-        local(wq, wg.at[:, pl.ds(0, 256)], 3),
+        local(wk, wkv.at[:, pl.ds(0, 128)], 1),
+        local(wv, wkv.at[:, pl.ds(128, 128)], 2),
         local(row_table.at[sp], rows_tab, 4),
         local(tokens.at[pl.ds(third, third)], xs.at[pl.ds(third, third)], 5),
         local(tokens.at[pl.ds(2 * third, third)], xs.at[pl.ds(2 * third, third)], 6),
+        local(wq, wqg, 3),
         local(lwq, wl.at[:, pl.ds(0, 256)], 7),
         local(lwk, wl.at[:, pl.ds(256, 128)], 8),
         local(lwv, wl.at[:, pl.ds(384, 128)], 9),
@@ -166,6 +167,7 @@
     ]
     for load in loads:
         load.start()
+    loads = dict(zip((0, 1, 2, 4, 5, 6, 3, 7, 8, 9, 10, 11), loads))
 
     barrier = pltpu.get_barrier_semaphore()
     peers = [q_peer(1), q_peer(2), q_peer(3), kv_peer(1), kv_peer(3), sp_peer(1), sp_peer(NSP - 1)]
@@ -182,9 +184,16 @@
     first_half = lax.rem(lane, 64) < 32
 
     def norm(r):
-        block = xs[pl.ds(r * third, third), :].astype(F32)
-        mean = jnp.mean(block * block, axis=-1, keepdims=True)
-        xn[pl.ds(r * third, third), :] = (block * lax.rsqrt(mean + EPSILON) * gain[...]).astype(BF)
+        for c in range(third // CHUNK):
+            rows = pl.ds(r * third + c * CHUNK, CHUNK)
+            squares = jnp.zeros((CHUNK, HEAD), F32)
+            for j in range(D // HEAD):
+                part = xs[rows, pl.ds(j * HEAD, HEAD)].astype(F32)
+                squares += part * part
+            factor = lax.rsqrt(jnp.sum(squares, axis=-1, keepdims=True) / D + EPSILON)
+            for j in range(D // HEAD):
+                cols = pl.ds(j * HEAD, HEAD)
+                xn[rows, cols] = (xs[rows, cols].astype(F32) * factor * gain[:, cols]).astype(BF)
 
     def rope(u, gain_row, r):
         mean = jnp.mean(u * u, axis=-1, keepdims=True)
@@ -199,25 +208,29 @@
 
         return (u * table(0) + swapped * table(1)).astype(BF)
 
-    def project_grid(r):
+    def project_keys(r):
         rows = pl.ds(r * third, third)
-        p = dot(xn[rows, :], wg[...])
-        kall[0, rows, :] = rope(p[:, 256:384], gain_k[...], r)
-        vall[0, pl.ds(0, HEAD), rows] = p[:, 384:512].T.astype(BF)
+        p = dot(xn[rows, :], wkv[...])
+        kall[0, rows, :] = rope(p[:, 0:128], gain_k[...], r)
+        vall[0, pl.ds(0, HEAD), rows] = p[:, 128:256].T.astype(BF)
+
+    def project_queries(r):
+        rows = pl.ds(r * third, third)
+        p = dot(xn[rows, :], wqg[...])
         scaled = gain_q[...] * SCORE
         qr[0, rows, :] = rope(p[:, 0:128], scaled, r)
         qr[1, rows, :] = rope(p[:, 128:256], scaled, r)
 
     loads[0].wait()
     norm(0)
-    for i in (1, 2, 3, 4, 5):
+    for i in (1, 2, 4, 5):
         loads[i].wait()
     norm(1)
-    project_grid(0)
+    project_keys(0)
     loads[6].wait()
     norm(2)
-    project_grid(1)
-    project_grid(2)
+    project_keys(1)
+    project_keys(2)
 
     pl.semaphore_wait(barrier, len(peers))
     value_rows = pl.ds(0, HEAD)
@@ -246,6 +259,9 @@
         send(*args)
     k_relay, v_relay = k_copy(3, 2, 4, 1), v_copy(1, 2, 5, 3)
 
+    loads[3].wait()
+    for r in range(3):
+        project_queries(r)
     ahead, behind, across = (lax.rem(x + d, SIDE) * 192 for d in (1, 3, 2))
     own = x * 192
     starts = (
@@ -353,6 +369,9 @@
         lax.fori_loop(0, units // 2, body, tops)
 
     attend(EARLY, 4, lambda i: i * 0, 1)
+
+    send_queries(0)
+    send_queries(1)
 
     for args in halos:
         remote(*args).wait_recv()
@@ -388,7 +407,7 @@
     send(*k_relay)
     remote(*v_down).wait_recv()
     send(*v_relay)
-    for k in range(BLOCKS):
+    for k in (2, 3):
         send_queries(k)
     remote(*k_down).wait_recv()
     remote(*v_up).wait_recv()
@@ -412,8 +431,8 @@
     def o_copy(k, s):
         return (osend.at[k, s], orecv.at[k, 4 - s], o_s.at[k, s], o_r.at[k, 4 - s], q_peer(s))
 
-    def send_results(k):
-        for s in (2, 1, 3):
+    def send_results(k, *targets):
+        for s in targets:
             for i in range(3):
                 osend[k, s, i] = packed(k * 10 + place[s] + i)
             send(*o_copy(k, s))
@@ -441,9 +460,8 @@
         one = jnp.concatenate([merged[0], merged[1][:64]], axis=0)
         two = jnp.concatenate([merged[1][64:], merged[2]], axis=0)
         features = jnp.concatenate([one, two, gather(lo, k)], axis=1)
-        for c in range(2):
-            keep[k, c] = dot(features[c * 96 : c * 96 + 96], wo[...])
-        dsend[k] = keep[k, 1 - core].astype(BF)
+        keep[k] = dot(features, wo[...])
+        dsend[k] = keep[k, pl.ds(pl.multiple_of((1 - core) * 96, 16), 96), :].astype(BF)
         send(*d_copy(k))
 
     def d_copy(k):
@@ -459,7 +477,7 @@
 
     def summed(k):
         remote(*d_copy(k)).wait_recv()
-        return keep[k, core] + drecv[k].astype(F32)
+        return keep[k, pl.ds(pl.multiple_of(core * 96, 16), 96), :] + drecv[k].astype(F32)
 
     def scatter(k):
         total = summed(k)
@@ -496,12 +514,15 @@
         else:
             wait_queries(k, 1 if k % 2 == 0 else 3)
         wait_queries(k, 2)
-        attend(k * 10, TILES, lambda i: i, SIDE)
-        send_results(k)
+        attend(k * 10, 3, lambda i: i, SIDE)
+        send_results(k, 2, 1)
         if k < 2:
             relay_queries(k + 2)
         if k > 0:
             merge(k - 1)
+        attend(k * 10 + 6, 2, lambda i: i, SIDE)
+        send_results(k, 3)
+        if k > 0:
             scatter(k - 1)
     merge(3)
     scatter(3)
@@ -537,7 +558,8 @@
         scratch_shapes=[
             pltpu.VMEM((ROWS, D), BF),
             pltpu.VMEM((ROWS, D), BF),
-            pltpu.VMEM((D, 512), BF),
+            pltpu.VMEM((D, 256), BF),
+            pltpu.VMEM((D, 256), BF),
             pltpu.VMEM((D, 512), BF),
             pltpu.VMEM((512, D), BF),
             pltpu.VMEM((2, 16, HEAD), F32),
@@ -557,7 +579,7 @@
             pltpu.VMEM((ROWS, 256), BF),
             pltpu.VMEM((BLOCKS, 4, 3, HEAD + 16, HEAD), BF),
             pltpu.VMEM((BLOCKS, 4, 3, HEAD + 16, HEAD), BF),
-            pltpu.VMEM((BLOCKS, 2, 96, D), F32),
+            pltpu.VMEM((BLOCKS, 192, D), F32),
             pltpu.VMEM((BLOCKS, 96, D), BF),
             pltpu.VMEM((BLOCKS, 96, D), BF),
             pltpu.VMEM((2, 96, D // 2), BF),

time: 70.1 us -> 67.8 us (0.967)
  Pallas kernels: 68.1 us -> 65.2 us
    pallas_call x1, Pallas kernels: 68.1 us -> 65.2 us  [shards(): pl.pallas_call(kernel, out_shape=jax.ShapeDtypeStruct((96, D), BF), in_sp...]
where the time goes in v2:
time: 67.8 us; the launch traced here: 67 us
  Pallas kernels  65.2 us (96%)
  local copies, waits for them, and re-layouts  1.77 us (3%)
    pallas_call x1, Pallas kernels, shards(): pl.pallas_call(kernel, out_shape=jax.ShapeDtypeStruct((96, D), BF), in_sp...  65.2 us
    unnamed x1, local copies, waits for them, and re-layouts  1.77 us

profile of v2, /device:TPU:1, one launch (start us, length us, event | category | flops | bytes accessed | tf_op | source)
XLA Modules:
  0.0 67.0 jit_solution(2713943216481961420)
XLA Ops:
  0.0 65.2 %shard_map.145 = bf16[96,2048]{1,0:T(8,128)(2,1)} custom-call(bf16[768,2048]{1,0:T(8,128)(2,1)} %tokens.1, f32[1,2048]{1,0:T(1,128)} %bitcast.3, bf16[2048,256]{1,0:T(8,128)(2,1)} %wq.1, bf16[2048,128]{1,0:T(8,128)(2,1)} %wk.1, bf16[2048,128]{1,0:T(8,128)(2,1)} %wv.1, f32[1,128]{1,0:T(1,128)} %bitcast.4, f32[1,128]{1,0:T(1,128)} %bitcast.5, ...), custom_call_target="tpu_custom_call" | custom-call | tf_op jit(solution)/shard_map/pallas_call | solution.py:553
  65.2 1.8 %copy.17 = bf16[96,2048]{1,0:T(8,128)(2,1)} copy(bf16[96,2048]{1,0:T(8,128)(2,1)} %shard_map.145) | data formatting | bytes 786432

commit v3 on v2

--- a/solution.py
+++ b/solution.py
@@ -165,9 +165,9 @@
         local(wog, wo.at[pl.ds(0, 256)], 10),
         local(wol, wo.at[pl.ds(256, 256)], 11),
     ]
-    for load in loads:
-        load.start()
     loads = dict(zip((0, 1, 2, 4, 5, 6, 3, 7, 8, 9, 10, 11), loads))
+    for i in (0, 1, 2, 4, 5, 6):
+        loads[i].start()
 
     barrier = pltpu.get_barrier_semaphore()
     peers = [q_peer(1), q_peer(2), q_peer(3), kv_peer(1), kv_peer(3), sp_peer(1), sp_peer(NSP - 1)]
@@ -222,9 +222,12 @@
         qr[1, rows, :] = rope(p[:, 128:256], scaled, r)
 
     loads[0].wait()
+    loads[3].start()
     norm(0)
     for i in (1, 2, 4, 5):
         loads[i].wait()
+    for i in (7, 8, 9, 10, 11):
+        loads[i].start()
     norm(1)
     project_keys(0)
     loads[6].wait()
@@ -300,6 +303,9 @@
         args = q_copy(qs.at[k], k, slot, 0, 1)
         remote(*args).wait_recv()
 
+    for k in range(BLOCKS):
+        send_queries(k)
+
     for i in (7, 8, 9):
         loads[i].wait()
     for r in range(3):
@@ -324,57 +330,58 @@
     for args in halos:
         send(*args)
 
-    def attend(base, tiles, slots, count):
+    def attend(base, tiles, slots, count, tops=None, following=None):
         units = tiles * count // 2
 
         def where(u):
             halves = []
             for h in range(2):
                 index = 2 * u + h
-                halves.append((slots(index // tiles), base + 2 * lax.rem(index, tiles)))
+                halves.append((slots(index // tiles), base + lax.rem(index, tiles)))
             return halves
 
-        def scores(u, ref):
+        def scores(halves, ref):
             tops = []
-            for h, (t, g) in enumerate(where(u)):
-                queries = jnp.concatenate([qp[g], qp[g + 1]], axis=1)
+            for h, (t, g) in enumerate(halves):
+                queries = jnp.concatenate([qp[2 * g], qp[2 * g + 1]], axis=1)
                 s = dot(kall[t], queries)
                 ref[h] = s
                 tops.append(jnp.max(s, axis=0, keepdims=True))
             return tops
 
-        def weigh(u, ref, tops):
-            for h, (t, g) in enumerate(where(u)):
-                before = jnp.concatenate([m[g], m[g + 1]], axis=1)
+        def weigh(halves, ref, tops):
+            for h, (t, g) in enumerate(halves):
+                before = m[g]
                 top = jnp.maximum(before, tops[h])
                 factor = jnp.exp2(before - top)
                 weights = jnp.exp2(ref[h] - top).astype(BF)
                 result = dot(vall[t], weights)
-                for i in range(2):
-                    part = slice(i * 128, i * 128 + 128)
-                    m[g + i] = top[:, part]
-                    l[g + i] = l[g + i] * factor[:, part] + result[HEAD : HEAD + 1, part]
-                    o[g + i] = o[g + i] * factor[:, part] + result[:HEAD, part]
-
-        tops = scores(0, s0)
+                m[g] = top
+                l[g] = l[g] * factor + result[HEAD : HEAD + 1]
+                o[g] = o[g] * factor + result[:HEAD]
+
+        if tops is None:
+            tops = scores(where(0), s0)
 
         def body(i, tops):
             u = 2 * i
-            later = scores(u + 1, s1)
-            weigh(u, s0, tops)
-            tops = scores(jnp.minimum(u + 2, units - 1), s0)
-            weigh(u + 1, s1, later)
+            later = scores(where(u + 1), s1)
+            weigh(where(u), s0, tops)
+            after = where(jnp.minimum(u + 2, units - 1))
+            if following is not None:
+                last = (i + 1) // (units // 2)
+                after = [
+                    (t * (1 - last) + ft * last, g * (1 - last) + fg * last)
+                    for (t, g), (ft, fg) in zip(after, following)
+                ]
+            tops = scores(after, s0)
+            weigh(where(u + 1), s1, later)
             return tops
 
-        lax.fori_loop(0, units // 2, body, tops)
-
-    attend(EARLY, 4, lambda i: i * 0, 1)
-
-    send_queries(0)
-    send_queries(1)
-
-    for args in halos:
-        remote(*args).wait_recv()
+        return lax.fori_loop(0, units // 2, body, tops)
+
+    attend(EARLY // 2, 4, lambda i: i * 0, 1)
+
     wide = 3 * WINDOW
     row = lax.rem(lax.broadcasted_iota(jnp.int32, (2 * WINDOW, wide), 0), WINDOW)
     col = lax.broadcasted_iota(jnp.int32, (2 * WINDOW, wide), 1)
@@ -401,32 +408,39 @@
         lo[pl.ds(at, WINDOW), :] = jnp.concatenate([result[:WINDOW], result[WINDOW:]], axis=1).astype(BF)
         return carry
 
-    lax.fori_loop(0, blocks, banded, 0)
+    lax.fori_loop(1, blocks - 1, banded, 0)
 
     remote(*k_up).wait_recv()
     send(*k_relay)
     remote(*v_down).wait_recv()
     send(*v_relay)
-    for k in (2, 3):
-        send_queries(k)
     remote(*k_down).wait_recv()
     remote(*v_up).wait_recv()
-    attend(EARLY, 4, lambda i: 1 + 2 * i, 2)
+    attend(EARLY // 2, 4, lambda i: 1 + 2 * i, 2)
     relay_queries(0)
+    relay_queries(1)
+    for args in halos:
+        remote(*args).wait_recv()
+    lax.fori_loop(0, 2, lambda i, carry: banded(i * (blocks - 1), carry), 0)
     remote(*k_relay).wait_recv()
     remote(*v_relay).wait_recv()
-    attend(EARLY, 4, lambda i: i * 0 + 2, 1)
-    relay_queries(1)
+    attend(EARLY // 2, 4, lambda i: i * 0 + 2, 1)
+    relay_queries(2)
+    relay_queries(3)
+
+    def state(g):
+        lanes = pl.ds(g % 2 * HEAD, HEAD)
+        return m[g // 2, :, lanes], l[g // 2, :, lanes], o[g // 2, :, lanes]
 
     def packed(g):
-        total = l[g]
-        level = m[g] + jnp.log2(total)
+        top, total, result = state(g)
+        level = top + jnp.log2(total)
         high = level.astype(BF)
         rest = level - high.astype(F32)
         mid = rest.astype(BF)
         low = (rest - mid.astype(F32)).astype(BF)
         tail = jnp.concatenate([high, mid, low, jnp.zeros((13, HEAD), BF)], axis=0)
-        return jnp.concatenate([(o[g] / total).astype(BF), tail], axis=0)
+        return jnp.concatenate([(result * (1.0 / total)).astype(BF), tail], axis=0)
 
     def o_copy(k, s):
         return (osend.at[k, s], orecv.at[k, 4 - s], o_s.at[k, s], o_r.at[k, 4 - s], q_peer(s))
@@ -447,13 +461,13 @@
             for s in (1, 2, 3):
                 rows = orecv[k, s, i, pl.ds(HEAD, 16), :].astype(F32)
                 levels.append(rows[0:1] + rows[1:2] + rows[2:3])
-            total = l[g]
-            mine = m[g] + jnp.log2(total)
+            highest, total, result = state(g)
+            mine = highest + jnp.log2(total)
             top = functools.reduce(jnp.maximum, levels, mine)
             share = jnp.exp2(mine - top)
             shares = [jnp.exp2(level - top) for level in levels]
             whole = share + shares[0] + shares[1] + shares[2]
-            acc = o[g] * (share / (total * whole))
+            acc = result * (share / (total * whole))
             for s in (1, 2, 3):
                 acc += orecv[k, s, i, value_rows, :].astype(F32) * (shares[s - 1] / whole)
             merged.append(acc.T.astype(BF))
@@ -508,19 +522,22 @@
 
     for i in (10, 11):
         loads[i].wait()
+    def wait_block(k):
+        wait_queries(k, 1 if k % 2 == 0 else 3)
+        wait_queries(k, 2)
+
+    wait_block(0)
+    tops = None
     for k in range(BLOCKS):
-        if k == 0:
-            wait_queries(0, 1)
-        else:
-            wait_queries(k, 1 if k % 2 == 0 else 3)
-        wait_queries(k, 2)
-        attend(k * 10, 3, lambda i: i, SIDE)
+        tops = attend(k * 5, 3, lambda i: i, SIDE, tops, [(0, k * 5 + 3), (0, k * 5 + 4)])
         send_results(k, 2, 1)
-        if k < 2:
-            relay_queries(k + 2)
         if k > 0:
             merge(k - 1)
-        attend(k * 10 + 6, 2, lambda i: i, SIDE)
+        following = None
+        if k + 1 < BLOCKS:
+            wait_block(k + 1)
+            following = [(0, k * 5 + 5), (0, k * 5 + 6)]
+        tops = attend(k * 5 + 3, 2, lambda i: i, SIDE, tops, following)
         send_results(k, 3)
         if k > 0:
             scatter(k - 1)
@@ -568,9 +585,9 @@
             pltpu.VMEM((48, HEAD, HEAD), BF),
             pltpu.VMEM((SIDE, ROWS, HEAD), BF),
             pltpu.VMEM((SIDE, HEAD + 16, ROWS), BF),
-            pltpu.VMEM((48, 1, HEAD), F32),
-            pltpu.VMEM((48, 1, HEAD), F32),
-            pltpu.VMEM((48, HEAD, HEAD), F32),
+            pltpu.VMEM((24, 1, 2 * HEAD), F32),
+            pltpu.VMEM((24, 1, 2 * HEAD), F32),
+            pltpu.VMEM((24, HEAD, 2 * HEAD), F32),
             pltpu.VMEM((2, ROWS, 256), F32),
             pltpu.VMEM((2, ROWS, 256), F32),
             pltpu.VMEM((ROWS, 256), BF),

time: 67.8 us -> 62.5 us (0.922)
  Pallas kernels: 65.2 us -> 60.6 us
    pallas_call x1, Pallas kernels: 65.2 us -> 60.6 us  [shards(): pl.pallas_call(kernel, out_shape=jax.ShapeDtypeStruct((96, D), BF), in_sp...]
where the time goes in v3:
time: 62.5 us; the launch traced here: 62.4 us
  Pallas kernels  60.6 us (97%)
  local copies, waits for them, and re-layouts  1.77 us (3%)
    pallas_call x1, Pallas kernels, shards(): pl.pallas_call(kernel, out_shape=jax.ShapeDtypeStruct((96, D), BF), in_sp...  60.6 us
    unnamed x1, local copies, waits for them, and re-layouts  1.77 us

profile of v3, /device:TPU:1, one launch (start us, length us, event | category | flops | bytes accessed | tf_op | source)
XLA Modules:
  0.0 62.4 jit_solution(3684683646390970149)
XLA Ops:
  0.0 60.6 %shard_map.145 = bf16[96,2048]{1,0:T(8,128)(2,1)} custom-call(bf16[768,2048]{1,0:T(8,128)(2,1)} %tokens.1, f32[1,2048]{1,0:T(1,128)} %bitcast.3, bf16[2048,256]{1,0:T(8,128)(2,1)} %wq.1, bf16[2048,128]{1,0:T(8,128)(2,1)} %wk.1, bf16[2048,128]{1,0:T(8,128)(2,1)} %wv.1, f32[1,128]{1,0:T(1,128)} %bitcast.4, f32[1,128]{1,0:T(1,128)} %bitcast.5, ...), custom_call_target="tpu_custom_call" | custom-call | tf_op jit(solution)/shard_map/pallas_call | solution.py:570
  60.6 1.8 %copy.17 = bf16[96,2048]{1,0:T(8,128)(2,1)} copy(bf16[96,2048]{1,0:T(8,128)(2,1)} %shard_map.145) | data formatting | bytes 786432

commit v4 on v3

--- a/solution.py
+++ b/solution.py
@@ -303,7 +303,7 @@
         args = q_copy(qs.at[k], k, slot, 0, 1)
         remote(*args).wait_recv()
 
-    for k in range(BLOCKS):
+    for k in (0, 1):
         send_queries(k)
 
     for i in (7, 8, 9):
@@ -414,19 +414,19 @@
     send(*k_relay)
     remote(*v_down).wait_recv()
     send(*v_relay)
+    relay_queries(0)
+    relay_queries(1)
+    for k in (2, 3):
+        send_queries(k)
     remote(*k_down).wait_recv()
     remote(*v_up).wait_recv()
     attend(EARLY // 2, 4, lambda i: 1 + 2 * i, 2)
-    relay_queries(0)
-    relay_queries(1)
     for args in halos:
         remote(*args).wait_recv()
     lax.fori_loop(0, 2, lambda i, carry: banded(i * (blocks - 1), carry), 0)
     remote(*k_relay).wait_recv()
     remote(*v_relay).wait_recv()
     attend(EARLY // 2, 4, lambda i: i * 0 + 2, 1)
-    relay_queries(2)
-    relay_queries(3)
 
     def state(g):
         lanes = pl.ds(g % 2 * HEAD, HEAD)
@@ -527,11 +527,15 @@
         wait_queries(k, 2)
 
     wait_block(0)
+    relay_queries(2)
+    relay_queries(3)
     tops = None
     for k in range(BLOCKS):
         tops = attend(k * 5, 3, lambda i: i, SIDE, tops, [(0, k * 5 + 3), (0, k * 5 + 4)])
         send_results(k, 2, 1)
-        if k > 0:
+        if k > 1:
+            scatter(k - 2)
+        if k == BLOCKS - 1:
             merge(k - 1)
         following = None
         if k + 1 < BLOCKS:
@@ -539,8 +543,10 @@
             following = [(0, k * 5 + 5), (0, k * 5 + 6)]
         tops = attend(k * 5 + 3, 2, lambda i: i, SIDE, tops, following)
         send_results(k, 3)
-        if k > 0:
+        if k == BLOCKS - 1:
             scatter(k - 1)
+        elif k > 0:
+            merge(k - 1)
     merge(3)
     scatter(3)
     for copy in sends:

time: 62.5 us -> 59.6 us (0.954)
  Pallas kernels: 60.6 us -> 57.6 us
    pallas_call x1, Pallas kernels: 60.6 us -> 57.6 us  [shards(): pl.pallas_call(kernel, out_shape=jax.ShapeDtypeStruct((96, D), BF), in_sp...]
where the time goes in v4:
time: 59.6 us; the launch traced here: 59.4 us
  Pallas kernels  57.6 us (97%)
  local copies, waits for them, and re-layouts  1.77 us (3%)
    pallas_call x1, Pallas kernels, shards(): pl.pallas_call(kernel, out_shape=jax.ShapeDtypeStruct((96, D), BF), in_sp...  57.6 us
    unnamed x1, local copies, waits for them, and re-layouts  1.77 us

profile of v4, /device:TPU:1, one launch (start us, length us, event | category | flops | bytes accessed | tf_op | source)
XLA Modules:
  0.0 59.4 jit_solution(11939829600069620397)
XLA Ops:
  0.0 57.6 %shard_map.145 = bf16[96,2048]{1,0:T(8,128)(2,1)} custom-call(bf16[768,2048]{1,0:T(8,128)(2,1)} %tokens.1, f32[1,2048]{1,0:T(1,128)} %bitcast.3, bf16[2048,256]{1,0:T(8,128)(2,1)} %wq.1, bf16[2048,128]{1,0:T(8,128)(2,1)} %wk.1, bf16[2048,128]{1,0:T(8,128)(2,1)} %wv.1, f32[1,128]{1,0:T(1,128)} %bitcast.4, f32[1,128]{1,0:T(1,128)} %bitcast.5, ...), custom_call_target="tpu_custom_call" | custom-call | tf_op jit(solution)/shard_map/pallas_call | solution.py:576
  57.6 1.8 %copy.17 = bf16[96,2048]{1,0:T(8,128)(2,1)} copy(bf16[96,2048]{1,0:T(8,128)(2,1)} %shard_map.145) | data formatting | bytes 786432

commit v5 on v4

--- a/solution.py
+++ b/solution.py
@@ -303,8 +303,7 @@
         args = q_copy(qs.at[k], k, slot, 0, 1)
         remote(*args).wait_recv()
 
-    for k in (0, 1):
-        send_queries(k)
+    send_queries(0)
 
     for i in (7, 8, 9):
         loads[i].wait()
@@ -415,8 +414,7 @@
     remote(*v_down).wait_recv()
     send(*v_relay)
     relay_queries(0)
-    relay_queries(1)
-    for k in (2, 3):
+    for k in (1, 2, 3):
         send_queries(k)
     remote(*k_down).wait_recv()
     remote(*v_up).wait_recv()
@@ -424,6 +422,7 @@
     for args in halos:
         remote(*args).wait_recv()
     lax.fori_loop(0, 2, lambda i, carry: banded(i * (blocks - 1), carry), 0)
+    relay_queries(1)
     remote(*k_relay).wait_recv()
     remote(*v_relay).wait_recv()
     attend(EARLY // 2, 4, lambda i: i * 0 + 2, 1)

time: 59.6 us -> 57.7 us (0.968)
  Pallas kernels: 57.6 us -> 55.8 us
    pallas_call x1, Pallas kernels: 57.6 us -> 55.8 us  [shards(): pl.pallas_call(kernel, out_shape=jax.ShapeDtypeStruct((96, D), BF), in_sp...]
where the time goes in v5:
time: 57.7 us; the launch traced here: 57.5 us
  Pallas kernels  55.8 us (97%)
  local copies, waits for them, and re-layouts  1.77 us (3%)
    pallas_call x1, Pallas kernels, shards(): pl.pallas_call(kernel, out_shape=jax.ShapeDtypeStruct((96, D), BF), in_sp...  55.8 us
    unnamed x1, local copies, waits for them, and re-layouts  1.77 us

profile of v5, /device:TPU:1, one launch (start us, length us, event | category | flops | bytes accessed | tf_op | source)
XLA Modules:
  0.0 57.5 jit_solution(17322834982054785493)
XLA Ops:
  0.0 55.8 %shard_map.145 = bf16[96,2048]{1,0:T(8,128)(2,1)} custom-call(bf16[768,2048]{1,0:T(8,128)(2,1)} %tokens.1, f32[1,2048]{1,0:T(1,128)} %bitcast.3, bf16[2048,256]{1,0:T(8,128)(2,1)} %wq.1, bf16[2048,128]{1,0:T(8,128)(2,1)} %wk.1, bf16[2048,128]{1,0:T(8,128)(2,1)} %wv.1, f32[1,128]{1,0:T(1,128)} %bitcast.4, f32[1,128]{1,0:T(1,128)} %bitcast.5, ...), custom_call_target="tpu_custom_call" | custom-call | tf_op jit(solution)/shard_map/pallas_call | solution.py:575
  55.8 1.8 %copy.17 = bf16[96,2048]{1,0:T(8,128)(2,1)} copy(bf16[96,2048]{1,0:T(8,128)(2,1)} %shard_map.145) | data formatting | bytes 786432

commit v6 on v5

--- a/solution.py
+++ b/solution.py
@@ -303,8 +303,6 @@
         args = q_copy(qs.at[k], k, slot, 0, 1)
         remote(*args).wait_recv()
 
-    send_queries(0)
-
     for i in (7, 8, 9):
         loads[i].wait()
     for r in range(3):
@@ -413,12 +411,14 @@
     send(*k_relay)
     remote(*v_down).wait_recv()
     send(*v_relay)
-    relay_queries(0)
-    for k in (1, 2, 3):
+    for k in (0, 1):
         send_queries(k)
     remote(*k_down).wait_recv()
     remote(*v_up).wait_recv()
     attend(EARLY // 2, 4, lambda i: 1 + 2 * i, 2)
+    relay_queries(0)
+    for k in (2, 3):
+        send_queries(k)
     for args in halos:
         remote(*args).wait_recv()
     lax.fori_loop(0, 2, lambda i, carry: banded(i * (blocks - 1), carry), 0)

time: 57.7 us -> 59.5 us (1.031)
  Pallas kernels: 55.8 us -> 57.5 us
    pallas_call x1, Pallas kernels: 55.8 us -> 57.5 us  [shards(): pl.pallas_call(kernel, out_shape=jax.ShapeDtypeStruct((96, D), BF), in_sp...]
where the time goes in v6:
time: 59.5 us; the launch traced here: 59.3 us
  Pallas kernels  57.5 us (97%)
  local copies, waits for them, and re-layouts  1.77 us (3%)
    pallas_call x1, Pallas kernels, shards(): pl.pallas_call(kernel, out_shape=jax.ShapeDtypeStruct((96, D), BF), in_sp...  57.5 us
    unnamed x1, local copies, waits for them, and re-layouts  1.77 us

profile of v6, /device:TPU:1, one launch (start us, length us, event | category | flops | bytes accessed | tf_op | source)
XLA Modules:
  0.0 59.3 jit_solution(1562296227231884014)
XLA Ops:
  0.0 57.5 %shard_map.145 = bf16[96,2048]{1,0:T(8,128)(2,1)} custom-call(bf16[768,2048]{1,0:T(8,128)(2,1)} %tokens.1, f32[1,2048]{1,0:T(1,128)} %bitcast.3, bf16[2048,256]{1,0:T(8,128)(2,1)} %wq.1, bf16[2048,128]{1,0:T(8,128)(2,1)} %wk.1, bf16[2048,128]{1,0:T(8,128)(2,1)} %wv.1, f32[1,128]{1,0:T(1,128)} %bitcast.4, f32[1,128]{1,0:T(1,128)} %bitcast.5, ...), custom_call_target="tpu_custom_call" | custom-call | tf_op jit(solution)/shard_map/pallas_call | solution.py:575
  57.5 1.8 %copy.17 = bf16[96,2048]{1,0:T(8,128)(2,1)} copy(bf16[96,2048]{1,0:T(8,128)(2,1)} %shard_map.145) | data formatting | bytes 786432

commit v7 on v5

--- a/solution.py
+++ b/solution.py
@@ -414,11 +414,12 @@
     remote(*v_down).wait_recv()
     send(*v_relay)
     relay_queries(0)
-    for k in (1, 2, 3):
-        send_queries(k)
+    send_queries(1)
     remote(*k_down).wait_recv()
     remote(*v_up).wait_recv()
     attend(EARLY // 2, 4, lambda i: 1 + 2 * i, 2)
+    for k in (2, 3):
+        send_queries(k)
     for args in halos:
         remote(*args).wait_recv()
     lax.fori_loop(0, 2, lambda i, carry: banded(i * (blocks - 1), carry), 0)

time: 57.7 us -> 58.7 us (1.017)
  Pallas kernels: 55.8 us -> 56.7 us
    pallas_call x1, Pallas kernels: 55.8 us -> 56.7 us  [shards(): pl.pallas_call(kernel, out_shape=jax.ShapeDtypeStruct((96, D), BF), in_sp...]
where the time goes in v7:
time: 58.7 us; the launch traced here: 58.5 us
  Pallas kernels  56.7 us (97%)
  local copies, waits for them, and re-layouts  1.77 us (3%)
    pallas_call x1, Pallas kernels, shards(): pl.pallas_call(kernel, out_shape=jax.ShapeDtypeStruct((96, D), BF), in_sp...  56.7 us
    unnamed x1, local copies, waits for them, and re-layouts  1.77 us

profile of v7, /device:TPU:1, one launch (start us, length us, event | category | flops | bytes accessed | tf_op | source)
XLA Modules:
  0.0 58.5 jit_solution(11407158411218425437)
XLA Ops:
  0.0 56.7 %shard_map.145 = bf16[96,2048]{1,0:T(8,128)(2,1)} custom-call(bf16[768,2048]{1,0:T(8,128)(2,1)} %tokens.1, f32[1,2048]{1,0:T(1,128)} %bitcast.3, bf16[2048,256]{1,0:T(8,128)(2,1)} %wq.1, bf16[2048,128]{1,0:T(8,128)(2,1)} %wk.1, bf16[2048,128]{1,0:T(8,128)(2,1)} %wv.1, f32[1,128]{1,0:T(1,128)} %bitcast.4, f32[1,128]{1,0:T(1,128)} %bitcast.5, ...), custom_call_target="tpu_custom_call" | custom-call | tf_op jit(solution)/shard_map/pallas_call | solution.py:576
  56.7 1.8 %copy.17 = bf16[96,2048]{1,0:T(8,128)(2,1)} copy(bf16[96,2048]{1,0:T(8,128)(2,1)} %shard_map.145) | data formatting | bytes 786432
